TPU v7x, 32 devices: a whole 2x2x4 slice. The times are simulated.
32 devices in a mesh: fs: 16 (over z, y, x), tp: 2 (over core).
Axes of the slice: x: 2, y: 2, z: 4, core: 2. Of those that a mesh axis runs over, the one named last changes fastest.
Arguments:
- sequence_entries: bfloat16 [4096, 2048], P('fs', 'tp'), may hold values from -6 to 6
- former_norm_factor: float32 [2048], replicated, may hold values from 0.1 to 1.9
- conveyor_matrix: float32 [2048, 1536], P('fs', 'tp'), may hold values from -0.125 to 0.125
- conveyor_rescalers: float32 [1536], P('tp'), may hold values from 0.3 to 3
- blend_value_matrix: float32 [2048, 1536], P('fs', 'tp'), may hold values from -0.125 to 0.125
- blend_rescalers: float32 [1536], P('tp'), may hold values from 0.18 to 4.8, as said below
- blend_norm_factor: float32 [1536], P('tp'), may hold values from 0.1 to 1.9
- location_matrices: bfloat16 [24, 128, 128], P('tp'), may hold values from -0.5 to 0.5
- location_offsets: float32 [24, 128], P('tp'), may hold values from 0.1 to 1.9
- branch_emission_matrix: float32 [1536, 2048], P('tp', 'fs'), may hold values from -0.15625 to 0.15625
- emission_rescalers: float32 [2048], P('fs'), may hold values from 0.3 to 3
- latter_norm_factor: float32 [2048], replicated, may hold values from 0.1 to 1.9
- valve_matrix: float32 [2048, 5632], P('fs', 'tp'), may hold values from -0.125 to 0.125
- valve_rescalers: float32 [5632], P('tp'), may hold values from 0.3 to 3
- raising_matrix: float32 [2048, 5632], P('fs', 'tp'), may hold values from -0.125 to 0.125
- raising_rescalers: float32 [5632], P('tp'), may hold values from 0.3 to 3
- lowering_matrix: float32 [5632, 2048], P('tp', 'fs'), may hold values from -0.078125 to 0.078125
- lowering_rescalers: float32 [2048], P('fs'), may hold values from 0.3 to 3
Outputs:
- layer_out: bfloat16 [4096, 2048], P('fs', 'tp')
Inputs may be any that keep to these rules, and one draw needn't show every extreme that they name: `blend_rescalers`: positive column scales.
All inputs are finite; a program needn't handle non-finite values.
Results may differ from a plain program's by a relative error of at most 0.02.
Values may be sent and summed in bfloat16 or wider, within the bound.
A program may use at most 128 MiB of HBM per device.

v0:
```python
import jax
import jax.numpy as jnp
from jax import lax
from jax.sharding import PartitionSpec as P

EPS = 1e-06


def normalize(rows, gain):
    values = rows.astype(jnp.float32)
    factor = lax.rsqrt(jnp.mean(values * values, axis=-1, keepdims=True) + EPS)
    return (values * factor * gain).astype(jnp.bfloat16)


def elementwise_plus(left_rows, pieces):
    return (
        jnp.dot(left_rows, pieces[0], preferred_element_type=jnp.float32),
        jnp.dot(left_rows, pieces[1], preferred_element_type=jnp.float32),
    )


def project_cols(left_rows, scales, piece):
    return jnp.dot(left_rows, piece, preferred_element_type=jnp.float32) * scales


def on_device(
    sequence_entries,
    former_norm_factor,
    conveyor_matrix,
    conveyor_rescalers,
    blend_value_matrix,
    blend_rescalers,
    blend_norm_factor,
    location_matrices,
    location_offsets,
    branch_emission_matrix,
    emission_rescalers,
    latter_norm_factor,
    valve_matrix,
    valve_rescalers,
    raising_matrix,
    raising_rescalers,
    lowering_matrix,
    lowering_rescalers,
):
    out_scales, down_scales = (
        lax.all_gather(emission_rescalers, "fs", axis=0, tiled=True),
        lax.all_gather(lowering_rescalers, "fs", axis=0, tiled=True),
    )
    full_rows = lax.all_gather(sequence_entries, "tp", axis=1, tiled=True)
    own_width = sequence_entries.shape[1]
    own_start = lax.axis_index("tp") * own_width
    standardized_source = normalize(full_rows, former_norm_factor)
    conveyor_prior, stream_prior = elementwise_plus(
        standardized_source,
        (
            lax.all_gather(conveyor_matrix.astype(jnp.bfloat16), "fs", axis=0, tiled=True),
            lax.all_gather(blend_value_matrix.astype(jnp.bfloat16), "fs", axis=0, tiled=True),
        ),
    )
    conveyor_current = jax.nn.gelu(conveyor_prior * conveyor_rescalers)
    signal = jax.nn.gelu(stream_prior * blend_rescalers)
    total_sq = lax.psum(jnp.sum(signal * signal, axis=1), "tp")
    channels = signal.shape[1] * lax.axis_size("tp")
    signal_norm = (
        signal * lax.rsqrt(total_sq / channels + EPS)[:, None] * blend_norm_factor
    ).astype(jnp.bfloat16)
    local_groups = location_matrices.shape[0]
    block_len = location_matrices.shape[1]
    group_width = signal.shape[1] // local_groups
    lower_mask = jnp.tril(jnp.ones((block_len, block_len), bool))
    masked = jnp.where(lower_mask[None], location_matrices, jnp.zeros((), jnp.bfloat16))
    signal_blocks = signal_norm.reshape(-1, block_len, local_groups, group_width)
    location_blended = jnp.einsum(
        "gts,bsgd->btgd", masked, signal_blocks, preferred_element_type=jnp.float32
    )
    location_blended = location_blended + location_offsets.T[None, :, :, None]
    filtered_result = (conveyor_current * location_blended.reshape(conveyor_current.shape)).astype(
        jnp.bfloat16
    )
    mixer_terms = project_cols(
        filtered_result,
        out_scales,
        lax.all_gather(branch_emission_matrix.astype(jnp.bfloat16), "fs", axis=1, tiled=True),
    )
    summed = lax.psum(mixer_terms.astype(jnp.bfloat16), "tp").astype(jnp.float32)
    mid_rows = (full_rows.astype(jnp.float32) + summed).astype(jnp.bfloat16)
    mid_own = lax.dynamic_slice_in_dim(mid_rows, own_start, own_width, 1)
    ffn_in = normalize(mid_rows, latter_norm_factor)
    gate_half = valve_matrix.astype(jnp.bfloat16)
    up_half = raising_matrix.astype(jnp.bfloat16)
    whole_gate, whole_up = (
        lax.all_gather(gate_half, "fs", axis=0, tiled=True),
        lax.all_gather(up_half, "fs", axis=0, tiled=True),
    )
    pre_gate = jnp.dot(ffn_in, whole_gate, preferred_element_type=jnp.float32)
    pre_up = jnp.dot(ffn_in, whole_up, preferred_element_type=jnp.float32)
    hidden = (jax.nn.silu(pre_gate * valve_rescalers) * (pre_up * raising_rescalers)).astype(
        jnp.bfloat16
    )
    ffn_terms = project_cols(
        hidden,
        down_scales,
        lax.all_gather(lowering_matrix.astype(jnp.bfloat16), "fs", axis=1, tiled=True),
    )
    ffn_share = lax.psum_scatter(
        ffn_terms.astype(jnp.bfloat16), "tp", scatter_dimension=1, tiled=True
    ).astype(jnp.float32)
    return (mid_own.astype(jnp.float32) + ffn_share).astype(jnp.bfloat16)


def solution(mesh):
    return jax.shard_map(
        on_device,
        mesh=mesh,
        in_specs=(
            P("fs", "tp"),
            P(),
            P("fs", "tp"),
            P("tp"),
            P("fs", "tp"),
            P("tp"),
            P("tp"),
            P("tp", None, None),
            P("tp", None),
            P("tp", "fs"),
            P("fs"),
            P(),
            P("fs", "tp"),
            P("tp"),
            P("fs", "tp"),
            P("tp"),
            P("tp", "fs"),
            P("fs"),
        ),
        out_specs=P("fs", "tp"),
        check_vma=False,
    )
```

profile of v0, /device:TPU:0, one launch (start us, length us, event | category | flops | bytes accessed | tf_op | source)
XLA Modules:
  0.0 764.5 jit_solution(3299104337699982424)
XLA Ops:
  6.5 0.0 all-gather.10.cloned.1.call-start
  6.5 0.7 all-gather.10.cloned.1.call-update
  7.3 0.0 all-gather.14.cloned.1.call-start
  7.3 1.7 convert_element_type.64
  9.0 0.0 all-gather.14.cloned.1.call-update
  9.0 0.0 all-gather.12.cloned.1.call-start
  9.1 1.7 convert_element_type.63
  10.8 0.0 all-gather.12.cloned.1.call-update
  10.8 0.0 all-gather.16.cloned.1.call-start
  10.9 1.7 convert_element_type.67
  12.5 0.0 all-gather.16.cloned.1.call-update
  12.6 0.0 all-reduce.2.cloned.1.call-start
  12.6 0.0 copy-done.6
  12.6 42.5 %all-gather = f32[16,1,128]{2,1,0:T(1,128)S(1)} all-gather(f32[1,1,128]{2,1,0:T(1,128)S(1)} %bitcast.34), channel_id=1, replica_groups=mesh['fs'=16,'tp'=2] {'fs'}, dimensions={0}, use_global_device_ids=true | all-gather | bytes 8704 | tf_op jit(solution)/shard_map/all_gather | solution.py:47
  55.1 0.0 all-gather.10.cloned.1.call-done
  55.1 1.5 fusion.7
  56.7 0.0 copy-start.5
  56.7 0.0 copy-start.4
  56.7 35.8 %all-gather.14.cloned.1.call-done = bf16[2048,768]{1,0:T(8,128)(2,1)} async-done(((bf16[128,768]{1,0:T(8,128)(2,1)}), bf16[2048,768]{1,0:T(8,128)(2,1)}) %all-gather.14.cloned.1.call-update) | async-done | bytes 3145744 | tf_op jit(solution)/shard_map/all_gather | solution.py:58
  92.5 0.0 copy-done.10
  92.5 0.0 copy-done.12
  92.5 3.5 multiply_reduce_fusion
  96.0 0.0 copy-start.3
  96.0 2.6 psum.14
  98.6 0.0 copy-done.5
  98.6 0.1 multiply_convert_fusion
  98.8 0.2 copy.25
  99.0 0.1 reshape.40
  99.1 0.0 copy-done.4
  99.1 0.0 copy-done.3
  99.1 0.0 copy-start
  99.1 0.0 copy-start.13
  99.1 0.4 fusion.11
  99.5 0.6 copy.27
  100.1 0.1 copy.34
  100.2 0.3 copy.28
  100.4 61.3 %all-gather.12.cloned.1.call-done = bf16[2048,768]{1,0:T(8,128)(2,1)} async-done(((bf16[128,768]{1,0:T(8,128)(2,1)}), bf16[2048,768]{1,0:T(8,128)(2,1)}) %all-gather.12.cloned.1.call-update) | async-done | bytes 3145744 | tf_op jit(solution)/shard_map/all_gather | solution.py:57
  161.7 77.2 %all-gather.16.cloned.1.call-done = bf16[768,2048]{1,0:T(8,128)(2,1)} async-done(((bf16[768,128]{1,0:T(8,128)(2,1)}), bf16[768,2048]{1,0:T(8,128)(2,1)}) %all-gather.16.cloned.1.call-update) | async-done | bytes 3145744 | tf_op jit(solution)/shard_map/all_gather | solution.py:84
  238.9 6.2 fusion.3
  245.1 0.0 all-reduce.2.cloned.1.call-update
  245.1 0.0 all-gather.18.cloned.1.call-start
  245.2 1.0 convert_element_type.74
  246.1 0.0 all-gather.18.cloned.1.call-update
  246.2 0.0 copy-start.7
  246.2 0.0 all-gather.20.cloned.1.call-start
  246.2 2.4 convert_element_type.75
  248.6 0.0 all-gather.20.cloned.1.call-update
  248.6 0.0 copy-start.8
  248.7 0.0 copy-start.11
  248.7 0.0 all-gather.22.cloned.1.call-start
  248.7 0.9 convert_element_type.77
  249.7 0.0 all-gather.22.cloned.1.call-update
  249.7 0.0 reduce-scatter.2.cloned.1.call-start
  249.8 38.3 %all-gather.1 = f32[16,1,128]{2,1,0:T(1,128)S(1)} all-gather(f32[1,1,128]{2,1,0:T(1,128)S(1)} %bitcast.35), channel_id=1, replica_groups=mesh['fs'=16,'tp'=2] {'fs'}, dimensions={0}, use_global_device_ids=true | all-gather | bytes 8704 | tf_op jit(solution)/shard_map/all_gather | solution.py:48
  288.0 1.7 fusion.4
  289.8 118.3 %all-gather.18.cloned.1.call-done = bf16[2048,2816]{1,0:T(8,128)(2,1)} async-done(((bf16[128,2816]{1,0:T(8,128)(2,1)}), bf16[2048,2816]{1,0:T(8,128)(2,1)}) %all-gather.18.cloned.1.call-update) | async-done | bytes 11534352 | tf_op jit(solution)/shard_map/all_gather | solution.py:93
  408.1 0.0 copy-done.8
  408.1 9.1 %convolution_multiply_fusion.1 = f32[256,2816]{1,0:T(8,128)} fusion(bf16[2048,2816]{1,0:T(8,128)(2,1)} %all-gather.18.cloned.1.call-done, f32[2816]{0:T(1024)S(1)} %copy-done.8, bf16[256,2048]{1,0:T(8,128)(2,1)S(1)} %get-tuple-element.6, f32[2048]{0:T(1024)S(1)} %copy-done.11, f32[256]{0:T(256)S(1)} %add_rsqrt_fusion), kind=kOutput, calls=%fused_computation.2 | convolution fusion | flops 2955608064 | bytes 15486976 | tf_op jit(solution)/shard_map/dot_general | solution.py:96
  417.3 133.3 %all-gather.20.cloned.1.call-done = bf16[2048,2816]{1,0:T(8,128)(2,1)} async-done(((bf16[128,2816]{1,0:T(8,128)(2,1)}), bf16[2048,2816]{1,0:T(8,128)(2,1)}) %all-gather.20.cloned.1.call-update) | async-done | bytes 11534352 | tf_op jit(solution)/shard_map/all_gather | solution.py:94
  550.5 183.0 %all-gather.22.cloned.1.call-done = bf16[2816,2048]{1,0:T(8,128)(2,1)} async-done(((bf16[2816,128]{1,0:T(8,128)(2,1)}), bf16[2816,2048]{1,0:T(8,128)(2,1)}) %all-gather.22.cloned.1.call-update) | async-done | bytes 11534352 | tf_op jit(solution)/shard_map/all_gather | solution.py:104
  733.5 15.7 %fusion.2 = bf16[256,2048]{1,0:T(8,128)(2,1)} fusion(bf16[2816,2048]{1,0:T(8,128)(2,1)} %all-gather.22.cloned.1.call-done, f32[2048]{0:T(1024)S(1)} %bitcast.33, bf16[2048,2816]{1,0:T(8,128)(2,1)} %all-gather.20.cloned.1.call-done, f32[256,2816]{1,0:T(8,128)} %convolution_multiply_fusion.1, f32[2816]{0:T(1024)S(1)} %copy-done.9, ...), kind=kOutput, calls=%fused_computation.11 | convolution fusion | flops 5913772032 | bytes 28078080 | tf_op jit(solution)/shard_map/dot_general | solution.py:23
  749.2 0.0 reduce-scatter.2.cloned.1.call-update
  749.2 6.7 reduce-scatter.2.cloned.1.call-done
  755.9 2.0 add_convert_fusion
  (18 shorter events, 0.1 us)
Async XLA Ops:
  6.5 6.1 copy-start.6
  6.5 86.0 %copy-start.10 = (f32[2048]{0:T(1024)S(1)}, f32[2048]{0:T(1024)}, u32[]{:S(2)}) copy-start(f32[2048]{0:T(1024)} %param.19) | copy-start | bytes 24580
  6.5 86.0 %copy-start.12 = (f32[768]{0:T(1024)S(1)}, f32[768]{0:T(1024)}, u32[]{:S(2)}) copy-start(f32[768]{0:T(1024)} %param.23) | copy-start | bytes 9220
  6.5 48.6 %all-gather.10.cloned.1.call-start = ((), (), s32[]{:S(2)}) async-start(), calls=%async_computation.1 | async-start | bytes 1572864 | tf_op jit(solution)/shard_map/all_gather | solution.py:50
  7.3 85.3 %all-gather.14.cloned.1.call-start = ((), (), s32[]{:S(2)}) async-start(), calls=%async_computation.3 | async-start | bytes 3342336 | tf_op jit(solution)/shard_map/all_gather | solution.py:58
  9.0 152.7 %all-gather.12.cloned.1.call-start = ((), (), s32[]{:S(2)}) async-start(), calls=%async_computation.2 | async-start | bytes 3342336 | tf_op jit(solution)/shard_map/all_gather | solution.py:57
  10.8 228.1 %all-gather.16.cloned.1.call-start = ((), (), s32[]{:S(2)}) async-start(), calls=%async_computation.4 | async-start | bytes 3342336 | tf_op jit(solution)/shard_map/all_gather | solution.py:84
  12.6 275.5 %all-reduce.2.cloned.1.call-start = ((), (), s32[]{:S(2)}) async-start(), calls=%async_computation.5 | async-start | bytes 2097152 | tf_op jit(solution)/shard_map/psum | solution.py:86
  56.7 42.0 %copy-start.5 = (f32[768]{0:T(1024)S(1)}, f32[768]{0:T(1024)}, u32[]{:S(2)}) copy-start(f32[768]{0:T(1024)} %param.24) | copy-start | bytes 9220
  56.7 42.4 %copy-start.4 = (f32[12,128]{1,0:T(8,128)S(1)}, f32[12,128]{1,0:T(8,128)}, u32[]{:S(2)}) copy-start(f32[12,128]{1,0:T(8,128)} %param.26) | copy-start | bytes 18436
  96.0 3.1 copy-start.3
  99.1 139.8 %copy-start = (bf16[256,2048]{1,0:T(8,128)(2,1)S(1)}, bf16[256,2048]{1,0:T(8,128)(2,1)}, u32[]{:S(2)}) copy-start(bf16[256,2048]{1,0:T(8,128)(2,1)} %all-gather.10.cloned.1.call-done) | copy-start | bytes 3145732
  99.1 139.8 %copy-start.13 = (f32[768]{0:T(1024)S(1)}, f32[768]{0:T(1024)}, u32[]{:S(2)}) copy-start(f32[768]{0:T(1024)} %param.21) | copy-start | bytes 9220
  238.9 6.2 copy-start.1
  245.1 163.0 %all-gather.18.cloned.1.call-start = ((), (), s32[]{:S(2)}) async-start(), calls=%async_computation.6 | async-start | bytes 12255232 | tf_op jit(solution)/shard_map/all_gather | solution.py:93
  246.1 2.6 copy-start.2
  246.2 3.6 copy-start.7
  246.2 304.4 %all-gather.20.cloned.1.call-start = ((), (), s32[]{:S(2)}) async-start(), calls=%async_computation.7 | async-start | bytes 12255232 | tf_op jit(solution)/shard_map/all_gather | solution.py:94
  248.6 159.5 %copy-start.8 = (f32[2816]{0:T(1024)S(1)}, f32[2816]{0:T(1024)}, u32[]{:S(2)}) copy-start(f32[2816]{0:T(1024)} %param.31) | copy-start | bytes 33796
  248.7 159.5 %copy-start.11 = (f32[2048]{0:T(1024)S(1)}, f32[2048]{0:T(1024)}, u32[]{:S(2)}) copy-start(f32[2048]{0:T(1024)} %param.29) | copy-start | bytes 24580
  248.7 484.8 %all-gather.22.cloned.1.call-start = ((), (), s32[]{:S(2)}) async-start(), calls=%async_computation.8 | async-start | bytes 12255232 | tf_op jit(solution)/shard_map/all_gather | solution.py:104
  249.7 506.2 %reduce-scatter.2.cloned.1.call-start = ((), (), s32[]{:S(2)}) async-start(), calls=%async_computation.9 | async-start | bytes 1572864 | tf_op jit(solution)/shard_map/reduce_scatter | solution.py:106
  408.1 325.4 %copy-start.9 = (f32[2816]{0:T(1024)S(1)}, f32[2816]{0:T(1024)}, u32[]{:S(2)}) copy-start(f32[2816]{0:T(1024)} %param.33) | copy-start | bytes 33796
Sparse Core Ops, SparseCore 0:
  8.9 11.7 all-gather.9
  23.4 69.0 all-gather.13
  95.3 66.3 all-gather.11
  164.3 74.5 all-gather.15
  245.2 17.5 all-reduce.1
  265.5 142.6 all-gather.17
  410.9 139.6 all-gather.19
  553.2 180.2 all-gather.21
  749.3 6.5 reduce-scatter.1
where the time goes:
time: 765 us; the launch traced here: 764 us
  waiting for transfers between devices  616 us (81%)
  blocking collectives  83.3 us (11%)
  matrix products  34.8 us (5%)
  other arithmetic  14.9 us (2%)
  between operations  13.4 us (2%)
    all_gather x1, waiting for transfers between devices, on_device(): lax.all_gather(lowering_matrix.astype(jnp.bfloat16), 'fs', axis=1, tiled=...  183 us
    all_gather x1, waiting for transfers between devices, on_device(): lax.all_gather(up_half, 'fs', axis=0, tiled=True)  133 us
    all_gather x1, waiting for transfers between devices, on_device(): lax.all_gather(gate_half, 'fs', axis=0, tiled=True)  118 us
    all_gather x1, waiting for transfers between devices, on_device(): lax.all_gather(branch_emission_matrix.astype(jnp.bfloat16), 'fs', axis=1,...  77.2 us
    all_gather x1, waiting for transfers between devices, on_device(): lax.all_gather(conveyor_matrix.astype(jnp.bfloat16), 'fs', axis=0, tiled=...  61.3 us
    all_gather x1, blocking collectives, on_device(): lax.all_gather(emission_rescalers, 'fs', axis=0, tiled=True)  42.5 us
    all_gather x1, blocking collectives, on_device(): lax.all_gather(lowering_rescalers, 'fs', axis=0, tiled=True)  38.3 us
    all_gather x1, waiting for transfers between devices, on_device(): lax.all_gather(blend_value_matrix.astype(jnp.bfloat16), 'fs', axis=0, til...  35.8 us
  transfers between devices with their start and end apart: 9, of which 7 were waited for; matrix products, arithmetic and copies ran while one was open for 4% of the time, Pallas kernels for 0%

commit v1 on v0

--- a/solution.py
+++ b/solution.py
@@ -1,9 +1,368 @@
+import functools
+
 import jax
 import jax.numpy as jnp
 from jax import lax
+from jax.experimental import pallas as pl
+from jax.experimental.pallas import tpu as pltpu
 from jax.sharding import PartitionSpec as P
 
 EPS = 1e-06
+MESH = pl.DeviceIdType.MESH
+BF = jnp.bfloat16
+F32 = jnp.float32
+
+
+def layer_kernel(
+    dims,
+    x_in, g1, wc_in, wb_in, we_in, wv_in, wr_in, wl_in,
+    sc, sb, gb, loc, offs, g2, sv, sr,
+    out,
+    wc, wb, we, wv, wr, wl,
+    xa, xm, nrm, car, sgn, gat, hid, sq, part, half, rcore, rx, rz, dx_in, dz_in,
+    p1s, p1r, p1l, p2s, p2r, ags, agr, sqs, sqr, rss, rsr,
+):
+    rows, width, chan, block_len, group_width, total_chan = dims
+    fs = lax.axis_index("fs")
+    c = lax.axis_index("tp")
+    x = fs % 2
+    y = (fs // 2) % 2
+    zl = (fs // 4) % 2
+    zh = fs // 8
+    ai = x + 2 * zl
+
+    def dev(dx=0, dy=0, dzl=0, dzh=0, dc=0):
+        nx = 1 - x if dx else x
+        ny = 1 - y if dy else y
+        nzl = 1 - zl if dzl else zl
+        nzh = 1 - zh if dzh else zh
+        nc = 1 - c if dc else c
+        return {"fs": nzh * 8 + nzl * 4 + ny * 2 + nx, "tp": nc}
+
+    def blk(da):
+        return (1 - x if da & 1 else x) + 2 * (1 - zl if da & 2 else zl)
+
+    peers = [dev(dx=da & 1, dzl=da & 2, dc=dc) for da in range(4) for dc in range(2) if da or dc]
+    peers += [dev(dy=1), dev(dzh=1)]
+    barrier = pltpu.get_barrier_semaphore()
+    for peer in peers:
+        pl.semaphore_signal(barrier, inc=1, device_id=peer, device_id_type=MESH)
+    pl.semaphore_wait(barrier, len(peers))
+
+    def rcopy(src, dst, ss, rs, to):
+        return pltpu.make_async_remote_copy(
+            src_ref=src, dst_ref=dst, send_sem=ss, recv_sem=rs, device_id=to, device_id_type=MESH
+        )
+
+    pending = []
+
+    def go(copy):
+        copy.start()
+        pending.append(copy)
+        return copy
+
+    ins = (wc_in, wb_in, we_in, wv_in, wr_in, wl_in)
+    dst = (wc, wb, we, wv, wr, wl)
+    rowwise = (False, False, True, False, False, True)
+
+    def cell(m):
+        if rowwise[m]:
+            lanes = ins[m].shape[2]
+            return dst[m].at[zh, zl, :, pl.ds(pl.multiple_of((y * 2 + x) * lanes, lanes), lanes)]
+        return dst[m].at[zh, zl, y, x]
+
+    def plane(m, a, b):
+        if rowwise[m]:
+            lanes = 2 * ins[m].shape[2]
+            return dst[m].at[a, :, :, pl.ds(pl.multiple_of(b * lanes, lanes), lanes)]
+        return dst[m].at[a, :, b]
+
+    first = {}
+    second = {}
+
+    def phase1(m):
+        local = pltpu.make_async_copy(ins[m].at[ai], cell(m), p1l.at[m])
+        local.start()
+        copies = [
+            go(rcopy(ins[m].at[blk(da)], cell(m), p1s.at[m, da - 1], p1r.at[m, da - 1], dev(dx=da & 1, dzl=da & 2)))
+            for da in (3, 1, 2)
+        ]
+        first[m] = (local, copies)
+
+    def phase2(m):
+        local, copies = first[m]
+        local.wait()
+        for copy in copies:
+            copy.wait_recv()
+        own = plane(m, zh, y)
+        zcopy = go(rcopy(own, own, p2s.at[m, 0], p2r.at[m, 0], dev(dzh=1)))
+        ycopy = go(rcopy(own, own, p2s.at[m, 1], p2r.at[m, 1], dev(dy=1)))
+        second[m] = [zcopy, ycopy]
+
+    def forward(m):
+        second[m][0].wait_recv()
+        far = plane(m, 1 - zh, y)
+        second[m].append(go(rcopy(far, far, p2s.at[m, 2], p2r.at[m, 2], dev(dy=1))))
+
+    def ready(m):
+        second[m][1].wait_recv()
+        second[m][2].wait_recv()
+
+    hr = rows // 2
+    top, bottom = pl.ds(0, hr), pl.ds(hr, hr)
+
+    def gather_start(buf, k):
+        own = buf.at[c, ai]
+        z = go(rcopy(own, own, ags.at[k, 0], agr.at[k, 0], dev(dzl=1)))
+        xx = go(rcopy(own, own, ags.at[k, 1], agr.at[k, 1], dev(dx=1)))
+        core = go(rcopy(own, own, ags.at[k, 2], agr.at[k, 2], dev(dc=1)))
+        return [z, xx, core]
+
+    def gather_forward(buf, k, st):
+        z, xx, core = st
+        z.wait_recv()
+        zb = buf.at[c, blk(2)]
+        zbt = buf.at[c, blk(2), top]
+        d1 = go(rcopy(zbt, zbt, ags.at[k, 3], agr.at[k, 3], dev(dx=1)))
+        c1 = go(rcopy(zb, zb, ags.at[k, 4], agr.at[k, 4], dev(dc=1)))
+        xx.wait_recv()
+        xb = buf.at[c, blk(1)]
+        xbb = buf.at[c, blk(1), bottom]
+        d2 = go(rcopy(xbb, xbb, ags.at[k, 5], agr.at[k, 5], dev(dzl=1)))
+        c2 = go(rcopy(xb, xb, ags.at[k, 6], agr.at[k, 6], dev(dc=1)))
+        st += [d1, c1, d2, c2]
+
+    def gather_last(buf, k, st):
+        d1, c1, d2, c2 = st[3:]
+        d1.wait_recv()
+        d2.wait_recv()
+        db = buf.at[c, blk(3)]
+        st.append(go(rcopy(db, db, ags.at[k, 7], agr.at[k, 7], dev(dc=1))))
+
+    def norm_block(buf, gain, b):
+        total = jnp.zeros((rows, 1), F32)
+        for h in range(2):
+            v = buf[h, b].astype(F32)
+            total = total + jnp.sum(v * v, axis=-1, keepdims=True)
+        factor = lax.rsqrt(total / (2 * width) + EPS)
+        for h in range(2):
+            nrm[h] = (buf[h, b].astype(F32) * factor * gain[h]).astype(BF)
+
+    def project(w):
+        n = w.shape[-1]
+        return jnp.dot(nrm[0], w[0].reshape(width, n), preferred_element_type=F32) + jnp.dot(
+            nrm[1], w[1].reshape(width, n), preferred_element_type=F32
+        )
+
+    def emit(src, w, b):
+        v = src[b]
+        for h in range(2):
+            for q in range(2):
+                n = w.shape[-1]
+                part[h, b, :, q * n:(q + 1) * n] = jnp.dot(
+                    v, w[h, q], preferred_element_type=F32
+                ).astype(BF)
+
+    def scatter(k, src, w):
+        cores = {}
+        order = (3, 2, 1, 0)
+        for i, da in enumerate(order):
+            b = blk(da)
+            emit(src, w, b)
+            cores[da] = rcopy(part.at[1 - c, b], rcore.at[k, b], rss.at[k, i], rsr.at[k, i], dev(dc=1))
+            cores[da].start()
+
+        def combine(da):
+            b = blk(da)
+            cores[da].wait_recv()
+            half[k, b] = (part[c, b].astype(F32) + rcore[k, b].astype(F32)).astype(BF)
+
+        combine(3)
+        dxc = go(rcopy(half.at[k, blk(3), top], dx_in.at[k], rss.at[k, 4], rsr.at[k, 4], dev(dx=1)))
+        dzc = go(rcopy(half.at[k, blk(3), bottom], dz_in.at[k], rss.at[k, 5], rsr.at[k, 5], dev(dzl=1)))
+        combine(2)
+        zb = blk(2)
+        z1 = go(rcopy(half.at[k, zb, bottom], rz.at[k, bottom], rss.at[k, 6], rsr.at[k, 6], dev(dzl=1)))
+        combine(1)
+        xb = blk(1)
+        x1 = go(rcopy(half.at[k, xb, top], rx.at[k, top], rss.at[k, 7], rsr.at[k, 7], dev(dx=1)))
+        dxc.wait_recv()
+        half[k, zb, :hr] = (half[k, zb, :hr].astype(F32) + dx_in[k].astype(F32)).astype(BF)
+        z2 = go(rcopy(half.at[k, zb, top], rz.at[k, top], rss.at[k, 8], rsr.at[k, 8], dev(dzl=1)))
+        dzc.wait_recv()
+        half[k, xb, hr:] = (half[k, xb, hr:].astype(F32) + dz_in[k].astype(F32)).astype(BF)
+        x2 = go(rcopy(half.at[k, xb, bottom], rx.at[k, bottom], rss.at[k, 9], rsr.at[k, 9], dev(dx=1)))
+        cores[0].wait_recv()
+        for da in order:
+            cores[da].wait_send()
+        own = part[c, ai].astype(F32) + rcore[k, ai].astype(F32)
+        for copy in (z1, x1, z2, x2):
+            copy.wait_recv()
+        return own + rz[k].astype(F32) + rx[k].astype(F32)
+
+    mine = pltpu.make_async_copy(x_in, xa.at[c, ai], p1l.at[6])
+    mine.start()
+    phase1(0)
+    phase1(1)
+    mine.wait()
+    st1 = gather_start(xa, 0)
+    phase2(0)
+    phase2(1)
+    gather_forward(xa, 0, st1)
+    for m in (2, 3, 4, 5):
+        phase1(m)
+    gather_last(xa, 0, st1)
+    forward(0)
+    forward(1)
+    for m in (2, 3, 4, 5):
+        phase2(m)
+    ready(0)
+    ready(1)
+    core_of = {0: 2, 2: 4, 1: 6, 3: 7}
+    slot = ai * 2 + c
+    for da in (0, 2, 1, 3):
+        b = blk(da)
+        st1[core_of[da]].wait_recv()
+        norm_block(xa, g1, b)
+        car[b] = jax.nn.gelu(project(wc) * sc[...])
+        signal = jax.nn.gelu(project(wb) * sb[...])
+        sgn[b] = (signal * gb[...]).astype(BF)
+        sq[slot, b] = lax.dot_general(
+            jnp.ones((8, chan), F32), signal * signal, (((1,), (1,)), ((), ())),
+            precision=lax.Precision.HIGHEST, preferred_element_type=F32,
+        )
+    squares = []
+    for da in range(4):
+        for dc in range(2):
+            if da or dc:
+                i = da * 2 + dc - 1
+                squares.append(
+                    go(rcopy(sq.at[slot], sq.at[slot], sqs.at[i], sqr.at[i], dev(dx=da & 1, dzl=da & 2, dc=dc)))
+                )
+    forward(2)
+    ready(2)
+    for copy in squares:
+        copy.wait_recv()
+    groups = chan // group_width
+    lower = lax.broadcasted_iota(jnp.int32, (block_len, block_len), 0) >= lax.broadcasted_iota(
+        jnp.int32, (block_len, block_len), 1
+    )
+    lane = lax.broadcasted_iota(jnp.int32, (block_len, chan), 1)
+    for da in range(4):
+        b = blk(da)
+        total = sq[0, b]
+        for i in range(1, 8):
+            total = total + sq[i, b]
+        factor = lax.rsqrt(total / total_chan + EPS)
+        for s in range(rows // block_len):
+            span = slice(s * block_len, (s + 1) * block_len)
+            values = sgn[b, span]
+            mixed = jnp.zeros((block_len, chan), F32)
+            for g in range(groups):
+                mat = jnp.where(lower, loc[g].astype(F32), 0.0) * factor[0:1, span]
+                one = jnp.dot(mat.astype(BF), values, preferred_element_type=F32)
+                inside = (lane >= g * group_width) & (lane < (g + 1) * group_width)
+                mixed = jnp.where(inside, one, mixed)
+            gat[b, span] = (car[b, span] * (mixed + offs[...])).astype(BF)
+    summed = scatter(0, gat, we)
+    xm[c, ai] = (xa[c, ai].astype(F32) + summed).astype(BF)
+    st2 = gather_start(xm, 1)
+    forward(3)
+    forward(4)
+    gather_forward(xm, 1, st2)
+    gather_last(xm, 1, st2)
+    ready(3)
+    ready(4)
+    for da in (0, 2, 1, 3):
+        b = blk(da)
+        st2[core_of[da]].wait_recv()
+        norm_block(xm, g2, b)
+        gate = project(wv) * sv[...]
+        up = project(wr) * sr[...]
+        hid[b] = (jax.nn.silu(gate) * up).astype(BF)
+    forward(5)
+    ready(5)
+    summed = scatter(1, hid, wl)
+    out[...] = (xm[c, ai].astype(F32) + summed).astype(BF)
+    for copy in pending:
+        copy.wait_send()
+
+
+def on_device_fused(
+    sequence_entries, former_norm_factor, conveyor_matrix, conveyor_rescalers,
+    blend_value_matrix, blend_rescalers, blend_norm_factor, location_matrices,
+    location_offsets, branch_emission_matrix, emission_rescalers, latter_norm_factor,
+    valve_matrix, valve_rescalers, raising_matrix, raising_rescalers,
+    lowering_matrix, lowering_rescalers,
+):
+    parts = 4
+    fs = lax.axis_index("fs")
+    ai = fs % 2 + 2 * ((fs // 4) % 2)
+    rows, width = sequence_entries.shape
+    depth = conveyor_matrix.shape[0]
+    chan = conveyor_matrix.shape[1] // parts
+    ff = valve_matrix.shape[1] // parts
+    groups = location_matrices.shape[0] // parts
+    block_len = location_matrices.shape[1]
+    group_width = chan // groups
+    total_chan = conveyor_matrix.shape[1] * lax.axis_size("tp")
+    cols = branch_emission_matrix.shape[1]
+
+    def by_columns(w):
+        return w.astype(BF).reshape(depth, parts, -1).transpose(1, 0, 2)
+
+    def by_rows(w, scale):
+        return (w * scale[None, :]).astype(BF).reshape(parts, -1, cols)
+
+    def own(v):
+        n = v.shape[0] // parts
+        return lax.dynamic_slice_in_dim(v, ai * n, n, 0)
+
+    offs = jnp.repeat(own(location_offsets), group_width, axis=0).T
+    args = (
+        sequence_entries,
+        former_norm_factor.reshape(2, 1, width),
+        by_columns(conveyor_matrix),
+        by_columns(blend_value_matrix),
+        by_rows(branch_emission_matrix, emission_rescalers),
+        by_columns(valve_matrix),
+        by_columns(raising_matrix),
+        by_rows(lowering_matrix, lowering_rescalers),
+        own(conveyor_rescalers)[None],
+        own(blend_rescalers)[None],
+        own(blend_norm_factor)[None],
+        own(location_matrices),
+        offs,
+        latter_norm_factor.reshape(2, 1, width),
+        own(valve_rescalers)[None],
+        own(raising_rescalers)[None],
+    )
+    vm = pltpu.VMEM
+    dma = pltpu.SemaphoreType.DMA
+    cube = (2, 2, 2, 2, depth)
+    scratch = [
+        vm(cube + (chan,), BF), vm(cube + (chan,), BF), vm((2, 2, chan, 4 * cols), BF),
+        vm(cube + (ff,), BF), vm(cube + (ff,), BF), vm((2, 2, ff, 4 * cols), BF),
+        vm((2, 4, rows, width), BF), vm((2, 4, rows, width), BF), vm((2, rows, width), BF),
+        vm((4, rows, chan), F32), vm((4, rows, chan), BF), vm((4, rows, chan), BF),
+        vm((4, rows, ff), BF), vm((8, 4, 8, rows), F32),
+        vm((2, 4, rows, width), BF), vm((2, 4, rows, width), BF), vm((2, 4, rows, width), BF),
+        vm((2, rows, width), BF), vm((2, rows, width), BF),
+        vm((2, rows // 2, width), BF), vm((2, rows // 2, width), BF),
+        dma((6, 3)), dma((6, 3)), dma((7,)), dma((6, 3)), dma((6, 3)),
+        dma((2, 8)), dma((2, 8)), dma((7,)), dma((7,)), dma((2, 10)), dma((2, 10)),
+    ]
+    dims = (rows, width, chan, block_len, group_width, total_chan)
+    return pl.pallas_call(
+        functools.partial(layer_kernel, dims),
+        out_shape=jax.ShapeDtypeStruct((rows, width), BF),
+        in_specs=[pl.BlockSpec(memory_space=pltpu.VMEM)] * len(args),
+        out_specs=pl.BlockSpec(memory_space=pltpu.VMEM),
+        scratch_shapes=scratch,
+        compiler_params=pltpu.CompilerParams(
+            collective_id=0, has_side_effects=True, vmem_limit_bytes=63000000
+        ),
+    )(*args)
 
 
 def normalize(rows, gain):
@@ -110,8 +469,10 @@
 
 
 def solution(mesh):
+    sizes = dict(mesh.shape)
+    fused = sizes["tp"] == 2 and sizes["fs"] == 16
     return jax.shard_map(
-        on_device,
+        on_device_fused if fused else on_device,
         mesh=mesh,
         in_specs=(
             P("fs", "tp"),

time: 765 us -> 280 us (0.37)
  waiting for transfers between devices: 616 us -> 0 us
  Pallas kernels: 0 us -> 260 us
  blocking collectives: 83.3 us -> 0 us
  matrix products: 34.8 us -> 0 us
  local copies, waits for them, and re-layouts: 1.27 us -> 17.9 us
  between operations: 13.4 us -> 0.11 us
  other arithmetic: 14.9 us -> 1.67 us
    all_gather x7 -> x0, waiting for transfers between devices: 609 us -> none  [the longest x1 183 us: on_device(): lax.all_gather(lowering_matrix.astype(jnp.bfloat16), 'fs', axis=1, tiled=...]
    pallas_call x0 -> x1, Pallas kernels: none -> 260 us  [on_device_fused(): pl.pallas_call(functools.partial(layer_kernel, dims), out_shape=jax.Shape...]
    all_gather x2 -> x0, blocking collectives: 80.7 us -> none  [the longest x1 42.5 us: on_device(): lax.all_gather(emission_rescalers, 'fs', axis=0, tiled=True)]
    dot_general x5 -> x0, matrix products: 34.8 us -> none  [the longest x2 21.8 us: project_cols(): jnp.dot(left_rows, piece, preferred_element_type=jnp.float32) * scales]
    convert_element_type x8 -> x2, other arithmetic: 11.6 us -> 1.67 us  [by_rows(): return (w * scale[None, :]).astype(BF).reshape(parts, -1, cols)]
  transfers between devices with their start and end apart: 9 -> 0, of which waited for: 7 -> 0; matrix products, arithmetic and copies ran while one was open for 4% -> 0% of each run, Pallas kernels for 0% -> 0%
where the time goes in v1:
time: 280 us; the launch traced here: 279 us
  Pallas kernels  260 us (93%)
  local copies, waits for them, and re-layouts  17.9 us (6%)
    pallas_call x1, Pallas kernels, on_device_fused(): pl.pallas_call(functools.partial(layer_kernel, dims), out_shape=jax.Shape...  260 us
    dynamic_slice x7, local copies, waits for them, and re-layouts, own(): return lax.dynamic_slice_in_dim(v, ai * n, n, 0)  7.02 us

profile of v1, /device:TPU:0, one launch (start us, length us, event | category | flops | bytes accessed | tf_op | source)
XLA Modules:
  0.0 279.5 jit_solution(6905270505264508145)
XLA Ops:
  0.0 0.0 copy-start
  0.0 0.0 copy-start.7
  0.0 0.0 copy-start.5
  0.0 0.0 copy-start.4
  0.1 1.5 dynamic_slice.21
  1.5 1.4 dynamic_slice.22
  2.9 1.3 dynamic_slice.23
  4.2 0.7 constant_dynamic-slice_fusion
  4.9 0.8 dynamic_slice.26
  5.7 0.6 broadcast_in_dim.24.sv
  6.3 0.8 dynamic_slice.27
  7.1 0.6 broadcast_in_dim.25.sr
  7.7 0.8 copy.28
  8.4 0.0 copy-done
  8.4 0.0 copy-start.1
  8.4 0.6 constant_dynamic-slice_fusion.1.loc
  9.1 1.2 copy.20
  10.2 0.9 copy.21
  11.1 0.0 copy-done.4
  11.1 0.2 copy.22
  11.2 0.9 copy.23
  12.1 0.0 copy-done.7
  12.1 0.0 copy-done.5
  12.1 0.7 multiply_convert_fusion.1
  12.8 0.0 copy-done.1
  12.8 0.3 copy.24
  13.2 0.0 copy-start.2
  13.2 1.2 copy.25
  14.3 0.5 copy-done.2
  14.8 0.0 copy-start.6
  14.8 0.3 copy.26
  15.2 0.0 copy-start.3
  15.2 1.2 copy.27
  16.4 0.0 copy-done.6
  16.4 0.5 copy-done.3
  16.8 1.0 multiply_convert_fusion
  17.8 259.8 %shard_map.172 = bf16[256,1024]{1,0:T(8,128)(2,1)} custom-call(bf16[256,1024]{1,0:T(8,128)(2,1)} %x_in.1, f32[2,1,1024]{2,1,0:T(1,128)} %bitcast.29, bf16[4,128,192]{2,1,0:T(8,128)(2,1)} %bitcast.22, bf16[4,128,192]{2,1,0:T(8,128)(2,1)} %bitcast.23, bf16[4,192,128]{2,1,0:T(8,128)(2,1)} %bitcast.24, bf16[4,128,704]{2,1,0:T(8,128)(2,1)} %bitcast.17, ...), custom_call_target="tpu_custom_call" | custom-call | tf_op jit(solution)/shard_map/pallas_call | solution.py:356
  277.6 1.9 copy.30
  (1 shorter events, 0.0 us)
Async XLA Ops:
  0.0 8.4 %copy-start = (bf16[12,128,128]{2,1,0:T(8,128)(2,1)S(1)}, bf16[12,128,128]{2,1,0:T(8,128)(2,1)}, u32[]{:S(2)}) copy-start(bf16[12,128,128]{2,1,0:T(8,128)(2,1)} %param.25) | copy-start | bytes 1179652
  0.0 12.1 %copy-start.7 = (f32[128]{0:T(128)S(1)}, f32[128]{0:T(128)}, u32[]{:S(2)}) copy-start(f32[128]{0:T(128)} %param.28) | copy-start | bytes 1540
  0.0 12.1 %copy-start.5 = (f32[768,128]{1,0:T(8,128)S(1)}, f32[768,128]{1,0:T(8,128)}, u32[]{:S(2)}) copy-start(f32[768,128]{1,0:T(8,128)} %param.27) | copy-start | bytes 1179652
  0.0 11.1 %copy-start.4 = (f32[128,768]{1,0:T(8,128)S(1)}, f32[128,768]{1,0:T(8,128)}, u32[]{:S(2)}) copy-start(f32[128,768]{1,0:T(8,128)} %param.22) | copy-start | bytes 1179652
  8.4 4.4 %copy-start.1 = (f32[128,2816]{1,0:T(8,128)S(1)}, f32[128,2816]{1,0:T(8,128)}, u32[]{:S(2)}) copy-start(f32[128,2816]{1,0:T(8,128)} %param.30) | copy-start | bytes 4325380
  13.2 1.7 copy-start.2
  14.8 1.5 copy-start.6
  15.2 1.7 copy-start.3
